TPU v7x, 32 devices: a whole 2x2x4 slice. The times are simulated.
32 devices in a mesh: kv: 4 (over y, x), tp: 8 (over z, core).
Axes of the slice: x: 2, y: 2, z: 4, core: 2. Of those that a mesh axis runs over, the one named last changes fastest.
Arguments:
- tokens: bfloat16 [128, 4096], P(None, ('kv', 'tp')), may hold values from -41 to 41
- lengths: int32 [128], P('kv'), may hold values from 1 to 8192, 262144 in all
- retention_state: float32 [128, 16, 128, 256], P('kv', 'tp'), may hold values from -4 to 4
- mixer_gain: float32 [4096], P('kv'), may hold values from 0.1 to 1.9
- query_weight: bfloat16 [4096, 2048], P('kv', 'tp'), may hold values from -0.09375 to 0.09375
- key_weight: bfloat16 [4096, 2048], P('kv', 'tp'), may hold values from -0.09375 to 0.09375
- value_weight: bfloat16 [4096, 4096], P('kv', 'tp'), may hold values from -0.09375 to 0.09375
- gate_weight: bfloat16 [4096, 4096], P('kv', 'tp'), may hold values from -0.09375 to 0.09375
- output_weight: bfloat16 [4096, 4096], P('tp', 'kv'), may hold values from -0.125 to 0.125
- channel_gain: float32 [4096], P('kv'), may hold values from 0.1 to 1.9
- ffn_gate: bfloat16 [4096, 11264], P('kv', 'tp'), may hold values from -0.09375 to 0.09375
- ffn_up: bfloat16 [4096, 11264], P('kv', 'tp'), may hold values from -0.09375 to 0.09375
- ffn_down: bfloat16 [11264, 4096], P('tp', 'kv'), may hold values from -0.078125 to 0.078125
Outputs:
- layer_output: bfloat16 [128, 4096], P(None, ('kv', 'tp'))
- new_state: float32 [128, 16, 128, 256], P('kv', 'tp')
All inputs are finite; a program needn't handle non-finite values. No bound on the sum of `lengths` on one device may be relied on, other than what follows from the above.
Results may differ from a plain program's by a relative error of at most 0.022.
Values may be sent and summed in bfloat16 or wider, within the bound.
A program may use at most 64 MiB of HBM per device.

v0:
```python
import jax
import jax.numpy as jnp
from jax import lax
from jax.sharding import PartitionSpec as P

D = 4096
HEADS = 16
QK = 128


def rotate_heads(vectors, positions):
    half_dim = vectors.shape[-1] // 2
    frequency = 10000.0 ** (-jnp.arange(half_dim, dtype=jnp.float32) / half_dim)
    angles = positions.astype(jnp.float32)[:, None, None] * frequency
    cosine = jnp.cos(angles)
    sine_part = jnp.sin(angles)
    first_half = vectors[..., :half_dim]
    second = vectors[..., half_dim:]
    return jnp.concatenate(
        [first_half * cosine - second * sine_part, first_half * sine_part + second * cosine],
        axis=-1,
    )


def gathered_rows(columns):
    return lax.all_gather(columns, "tp", axis=1, tiled=True)


def owned_sums(partial_value, squares):
    raw_sums, totals = (
        lax.psum_scatter(
            partial_value.astype(jnp.bfloat16), "kv", scatter_dimension=0, tiled=True
        ).astype(jnp.float32),
        lax.psum_scatter(
            squares.astype(jnp.bfloat16), "kv", scatter_dimension=0, tiled=True
        ).astype(jnp.float32),
    )
    summed = raw_sums * lax.rsqrt(totals / D + 1e-06)[:, None]
    return summed


def every_sum(partial_value, squares):
    raw_sums, totals = (
        lax.psum(partial_value.astype(jnp.bfloat16), "kv").astype(jnp.float32),
        lax.psum(squares.astype(jnp.bfloat16), "kv").astype(jnp.float32),
    )
    summed = raw_sums * lax.rsqrt(totals / D + 1e-06)[:, None]
    return summed


def on_device(
    tokens,
    lengths,
    retention_state,
    mixer_gain,
    query_weight,
    key_weight,
    value_weight,
    gate_weight,
    output_weight,
    channel_gain,
    ffn_gate,
    ffn_up,
    ffn_down,
):
    feature_block = gathered_rows(tokens).astype(jnp.float32)
    squares = jnp.sum(feature_block * feature_block, axis=1)
    normed = (feature_block * mixer_gain).astype(jnp.bfloat16)
    partial_value = jnp.concatenate(
        [
            jnp.dot(normed, query_weight, preferred_element_type=jnp.float32),
            jnp.dot(normed, key_weight, preferred_element_type=jnp.float32),
            jnp.dot(normed, value_weight, preferred_element_type=jnp.float32),
            jnp.dot(normed, gate_weight, preferred_element_type=jnp.float32),
        ],
        axis=1,
    )
    owned_rows = owned_sums(partial_value, squares)
    local_heads = query_weight.shape[1] // QK
    q_width = query_weight.shape[1]
    v_width = value_weight.shape[1]
    head_width = v_width // local_heads
    seq_rows = owned_rows.shape[0]
    query_rows = rotate_heads(
        owned_rows[:, :q_width].reshape(seq_rows, local_heads, QK), lengths
    ).astype(jnp.bfloat16)
    key_rows = (
        rotate_heads(
            owned_rows[:, q_width : 2 * q_width].reshape(seq_rows, local_heads, QK), lengths
        )
        * QK ** (-0.5)
    ).astype(jnp.bfloat16)
    value_rows = (
        owned_rows[:, 2 * q_width : 2 * q_width + v_width]
        .astype(jnp.bfloat16)
        .reshape(seq_rows, local_heads, head_width)
    )
    gate_rows = owned_rows[:, 2 * q_width + v_width :]
    head_ids = (lax.axis_index("tp") * local_heads + jnp.arange(local_heads)).astype(jnp.float32)
    decay_rate = 1.0 - 2.0 ** (-5.0 - 10.0 * head_ids / (HEADS - 1))
    new_state = (
        decay_rate[None, :, None, None] * retention_state
        + key_rows.astype(jnp.float32)[..., :, None] * value_rows.astype(jnp.float32)[..., None, :]
    )
    retained = jnp.einsum(
        "bhk,bhkv->bhv", query_rows.astype(jnp.float32), new_state, precision=lax.Precision.HIGHEST
    )
    normalized = retained * lax.rsqrt(jnp.mean(retained * retained, axis=-1) + 1e-06)[..., None]
    merged = (normalized.reshape(seq_rows, v_width) * jax.nn.silu(gate_rows)).astype(jnp.bfloat16)
    mixed_part = jnp.dot(
        lax.all_gather(merged, "kv", axis=0, tiled=True),
        output_weight,
        preferred_element_type=jnp.float32,
    )
    mixed_cols = lax.psum_scatter(
        mixed_part.astype(jnp.bfloat16), "tp", scatter_dimension=1, tiled=True
    ).astype(jnp.float32)
    residual = (tokens.astype(jnp.float32) + mixed_cols).astype(jnp.bfloat16)
    block_two = gathered_rows(residual).astype(jnp.float32)
    squares_two = jnp.sum(block_two * block_two, axis=1)
    normed_two = (block_two * channel_gain).astype(jnp.bfloat16)
    partial_two = jnp.concatenate(
        [
            jnp.dot(normed_two, ffn_gate, preferred_element_type=jnp.float32),
            jnp.dot(normed_two, ffn_up, preferred_element_type=jnp.float32),
        ],
        axis=1,
    )
    hidden_units = ffn_gate.shape[1]
    summed = every_sum(partial_two, squares_two)
    hidden = (jax.nn.silu(summed[:, :hidden_units]) * summed[:, hidden_units:]).astype(jnp.bfloat16)
    down_part = jnp.dot(hidden, ffn_down, preferred_element_type=jnp.float32)
    down_sums = lax.psum_scatter(
        down_part.astype(jnp.bfloat16), "tp", scatter_dimension=1, tiled=True
    ).astype(jnp.float32)
    layer_output = (residual.astype(jnp.float32) + down_sums).astype(jnp.bfloat16)
    return (layer_output, new_state)


def solution(mesh):
    in_specs = (
        P(None, ("kv", "tp")),
        P("kv"),
        P("kv", "tp", None, None),
        P("kv"),
        P("kv", "tp"),
        P("kv", "tp"),
        P("kv", "tp"),
        P("kv", "tp"),
        P("tp", "kv"),
        P("kv"),
        P("kv", "tp"),
        P("kv", "tp"),
        P("tp", "kv"),
    )
    out_specs = (P(None, ("kv", "tp")), P("kv", "tp", None, None))
    return jax.shard_map(
        on_device, mesh=mesh, in_specs=in_specs, out_specs=out_specs, check_vma=False
    )
```

profile of v0, /device:TPU:0, one launch (start us, length us, event | category | flops | bytes accessed | tf_op | source)
XLA Modules:
  0.0 209.1 jit_solution(6467621606597267192)
XLA Ops:
  7.2 15.1 %all_gather.9 = bf16[128,1024]{1,0:T(8,128)(2,1)S(1)} all-gather(bf16[128,128]{1,0:T(8,128)(2,1)} %param.13), channel_id=1, replica_groups=mesh['kv'=4,'tp'=8] {'tp'}, dimensions={1}, use_global_device_ids=true | all-gather | bytes 294912 | tf_op jit(solution)/shard_map/all_gather | solution.py:26
  22.4 1.3 convolution_convert_fusion.6
  23.7 1.3 convolution_convert_fusion.7
  25.0 1.5 convolution_convert_fusion.5
  26.6 0.3 convolution_convert_fusion.4
  26.9 0.8 pad_maximum_fusion.1
  27.8 0.6 dynamic-slice
  29.2 10.0 %all-reduce = bf16[128]{0:T(256)(128)(2,1)S(1)} all-reduce(bf16[128]{0:T(256)(128)(2,1)S(1)} %fusion.2), channel_id=3, replica_groups=mesh['kv'=4,'tp'=8] {'kv'}, use_global_device_ids=true, to_apply=%region_2.0.clone | all-reduce | flops 128 | bytes 512
  39.2 0.1 multiply_cosine_fusion
  39.4 13.0 %reduce-scatter.8.cloned.1.call-done = bf16[32,1536]{1,0:T(8,128)(2,1)} async-done(((bf16[128,1536]{1,0:T(8,128)(2,1)}), bf16[32,1536]{1,0:T(8,128)(2,1)}) %reduce-scatter.8.cloned.1.call-update) | async-done | bytes 98320 | tf_op jit(solution)/shard_map/reduce_scatter | solution.py:31
  52.4 1.0 convert_multiply_fusion.5
  53.5 0.2 subtract_convert_fusion
  53.9 4.7 %multiply_add_fusion = f32[32,2,128,256]{3,2,1,0:T(8,128)S(1)} fusion(f32[32,2,128,256]{3,2,1,0:T(8,128)} %param.15, f32[32,2,256]{2,1,0:T(2,128)S(1)} %reshape.119, f32[32,2,128]{2,1,0:T(2,128)S(1)} %fusion.18, f32[2]{0:T(128)S(1)} %power_subtract_fusion), kind=kLoop, calls=%fused_computation | loop fusion | flops 6291456 | bytes 16875528 | tf_op jit(solution)/shard_map/add | solution.py:102
  58.6 2.8 %fusion.16 = f32[32,2,1,256]{3,2,1,0:T(1,128)S(1)} fusion(f32[32,2,128,256]{3,2,1,0:T(8,128)S(1)} %multiply_add_fusion, bf16[32,2,128,1]{2,1,0,3:T(2,128)(2,1)S(1)} %maximum_bitcast_fusion), kind=kOutput, calls=%fused_computation.34 | convolution fusion | flops 25165824 | bytes 8470528 | tf_op jit(solution)/shard_map/bhk,bhkv->bhv/dot_general | solution.py:105
  61.4 0.5 copy-done.1
  62.3 8.5 %all_gather.10 = bf16[128,512]{1,0:T(8,128)(2,1)S(1)} all-gather(bf16[32,512]{1,0:T(8,128)(2,1)S(1)} %multiply_convert_fusion), channel_id=1, replica_groups=mesh['kv'=4,'tp'=8] {'kv'}, dimensions={0}, use_global_device_ids=true | all-gather | bytes 163840 | tf_op jit(solution)/shard_map/all_gather | solution.py:111
  70.8 0.3 convolution_convert_fusion.3
  71.1 0.8 copy.17
  72.0 30.9 %reduce-scatter.10.cloned.1.call-done = bf16[128,128]{1,0:T(8,128)(2,1)} async-done(((bf16[1024,128]{1,0:T(8,128)(2,1)}), bf16[128,128]{1,0:T(8,128)(2,1)}) %reduce-scatter.10.cloned.1.call-update) | async-done | bytes 32784
  102.9 0.9 copy.18
  103.8 13.2 %all_gather.11 = bf16[128,1024]{1,0:T(8,128)(2,1)S(1)} all-gather(bf16[128,128]{1,0:T(8,128)(2,1)S(1)} %add_convert_fusion.1), channel_id=1, replica_groups=mesh['kv'=4,'tp'=8] {'tp'}, dimensions={1}, use_global_device_ids=true | all-gather | bytes 294912 | tf_op jit(solution)/shard_map/all_gather | solution.py:26
  117.0 0.6 convolution_convert_fusion
  117.6 0.6 convolution_convert_fusion.1
  118.2 0.9 pad_maximum_fusion
  119.4 10.2 %psum.15 = bf16[128]{0:T(256)(128)(2,1)S(1)} all-reduce(bf16[128]{0:T(256)(128)(2,1)S(1)} %fusion.4), channel_id=1, replica_groups=mesh['kv'=4,'tp'=8] {'kv'}, use_global_device_ids=true, to_apply=%region_7.8 | all-reduce | flops 128 | bytes 512 | tf_op jit(solution)/shard_map/psum | solution.py:45
  129.6 35.9 %all-reduce.3.cloned.1.call-done = bf16[128,2816]{1,0:T(8,128)(2,1)} async-done(((bf16[128,2816]{1,0:T(8,128)(2,1)}), bf16[128,2816]{1,0:T(8,128)(2,1)}) %all-reduce.3.cloned.1.call-update) | async-done | bytes 720912 | tf_op jit(solution)/shard_map/psum | solution.py:44
  165.5 1.3 convert_multiply_fusion
  166.8 2.4 %convolution_convert_fusion.2 = bf16[128,1024]{1,0:T(8,128)(2,1)S(1)} fusion(bf16[1408,1024]{1,0:T(8,128)(2,1)} %param.25, f32[128,2816]{1,0:T(8,128)S(1)} %convert_multiply_fusion), kind=kOutput, calls=%fused_computation.4 | convolution fusion | flops 370311168 | bytes 4587520 | tf_op jit(solution)/shard_map/dot_general | solution.py:132
  169.2 0.8 copy.19
  170.1 31.0 %reduce-scatter.12.cloned.1.call-done = bf16[128,128]{1,0:T(8,128)(2,1)} async-done(((bf16[1024,128]{1,0:T(8,128)(2,1)}), bf16[128,128]{1,0:T(8,128)(2,1)}) %reduce-scatter.12.cloned.1.call-update) | async-done | bytes 32784
  201.1 0.9 copy.20
  201.9 0.6 add_convert_fusion
  (47 shorter events, 1.2 us)
Async XLA Ops:
  7.2 109.9 %copy-start = (bf16[1024,1408]{1,0:T(8,128)(2,1)S(1)}, bf16[1024,1408]{1,0:T(8,128)(2,1)}, u32[]{:S(2)}) copy-start(bf16[1024,1408]{1,0:T(8,128)(2,1)} %param.24) | copy-start | bytes 8650756
  7.2 19.4 %copy-start.6 = (f32[1024]{0:T(1024)S(1)}, f32[1024]{0:T(1024)}, u32[]{:S(2)}) copy-start(f32[1024]{0:T(1024)} %param.16) | copy-start | bytes 12292
  7.2 45.2 %reduce-scatter.8.cloned.1.call-start = ((), (), s32[]{:S(2)}) async-start(), calls=%async_computation.3 | async-start | bytes 491520 | tf_op jit(solution)/shard_map/reduce_scatter | solution.py:31
  7.2 19.4 %copy-start.3 = (bf16[1024,512]{1,0:T(8,128)(2,1)S(1)}, bf16[1024,512]{1,0:T(8,128)(2,1)}, u32[]{:S(2)}) copy-start(bf16[1024,512]{1,0:T(8,128)(2,1)} %param.20) | copy-start | bytes 3145732
  22.4 5.4 %copy-start.9 = (u32[32]{0:T(128)S(1)}, u32[32]{0:T(128)}, u32[]{:S(2)}) copy-start(u32[32]{0:T(128)} %constant.45) | copy-start | bytes 388
  22.4 6.6 %copy-start.8 = (s32[32]{0:T(128)S(1)}, s32[32]{0:T(128)}, u32[]{:S(2)}) copy-start(s32[32]{0:T(128)} %param.14) | copy-start | bytes 388
  27.7 75.2 %reduce-scatter.10.cloned.1.call-start = ((), (), s32[]{:S(2)}) async-start(), calls=%async_computation.5 | async-start | bytes 294912
  58.6 3.4 %copy-start.1 = (f32[32,2,128,256]{3,2,1,0:T(8,128)}, f32[32,2,128,256]{3,2,1,0:T(8,128)S(1)}, u32[]{:S(2)}) copy-start(f32[32,2,128,256]{3,2,1,0:T(8,128)S(1)} %multiply_add_fusion) | copy-start | bytes 25165828
  58.6 12.2 %copy-start.4 = (bf16[512,1024]{1,0:T(8,128)(2,1)S(1)}, bf16[512,1024]{1,0:T(8,128)(2,1)}, u32[]{:S(2)}) copy-start(bf16[512,1024]{1,0:T(8,128)(2,1)} %param.21) | copy-start | bytes 3145732
  62.0 41.8 %copy-start.5 = (bf16[128,128]{1,0:T(8,128)(2,1)S(1)}, bf16[128,128]{1,0:T(8,128)(2,1)}, u32[]{:S(2)}) copy-start(bf16[128,128]{1,0:T(8,128)(2,1)} %param.13) | copy-start | bytes 98308
  62.0 55.0 %copy-start.7 = (f32[1024]{0:T(1024)S(1)}, f32[1024]{0:T(1024)}, u32[]{:S(2)}) copy-start(f32[1024]{0:T(1024)} %param.22) | copy-start | bytes 12292
  72.0 93.6 %all-reduce.3.cloned.1.call-start = ((), (), s32[]{:S(2)}) async-start(), calls=%async_computation.4 | async-start | bytes 1441792 | tf_op jit(solution)/shard_map/psum | solution.py:44
  103.7 13.9 %copy-start.2 = (bf16[1024,1408]{1,0:T(8,128)(2,1)S(1)}, bf16[1024,1408]{1,0:T(8,128)(2,1)}, u32[]{:S(2)}) copy-start(bf16[1024,1408]{1,0:T(8,128)(2,1)} %param.23) | copy-start | bytes 8650756
  119.2 81.9 %reduce-scatter.12.cloned.1.call-start = ((), (), s32[]{:S(2)}) async-start(), calls=%async_computation.6 | async-start | bytes 294912
Sparse Core Ops, SparseCore 0:
  27.8 24.5 reduce-scatter.7
  72.1 30.7 reduce-scatter.9
  119.3 46.1 all-reduce.2
  170.2 30.7 reduce-scatter.11
where the time goes:
time: 210 us; the launch traced here: 209 us
  waiting for transfers between devices  111 us (53%)
  blocking collectives  57.1 us (27%)
  between operations  14.7 us (7%)
  matrix products  11.2 us (5%)
  other arithmetic  10.4 us (5%)
  local copies, waits for them, and re-layouts  4.66 us (2%)
    unnamed x6, waiting for transfers between devices  61.9 us
    psum x1, waiting for transfers between devices, every_sum(): lax.psum(partial_value.astype(jnp.bfloat16), 'kv').astype(jnp.float32)  35.9 us
    all_gather x2, blocking collectives, gathered_rows(): return lax.all_gather(columns, 'tp', axis=1, tiled=True)  28.4 us
    reduce_scatter x1, waiting for transfers between devices, owned_sums(): lax.psum_scatter(partial_value.astype(jnp.bfloat16), 'kv', scatter_dimens...  13 us
    psum x1, blocking collectives, every_sum(): lax.psum(squares.astype(jnp.bfloat16), 'kv').astype(jnp.float32)  10.2 us
    unnamed x1, blocking collectives  9.95 us
    all_gather x1, blocking collectives, on_device(): lax.all_gather(merged, 'kv', axis=0, tiled=True)  8.51 us
    add x1, other arithmetic, on_device(): decay_rate[None, :, None, None] * retention_state  4.67 us
  transfers between devices with their start and end apart: 4, of which 4 were waited for; matrix products, arithmetic and copies ran while one was open for 1% of the time, Pallas kernels for 0%

commit v1 on v0

--- a/solution.py
+++ b/solution.py
@@ -1,11 +1,17 @@
+import functools
+
 import jax
 import jax.numpy as jnp
+import numpy as np
 from jax import lax
+from jax.experimental import pallas as pl
+from jax.experimental.pallas import tpu as pltpu
 from jax.sharding import PartitionSpec as P
 
 D = 4096
 HEADS = 16
 QK = 128
+LANES = 128
 
 
 def rotate_heads(vectors, positions):
@@ -137,6 +143,355 @@
     return (layer_output, new_state)
 
 
+MESH_ID = pl.DeviceIdType.MESH
+VMEM_LIMIT = 48 * 1024 * 1024
+
+
+def greet(axes):
+    barrier = pltpu.get_barrier_semaphore()
+    for axis, count, me in axes:
+        for step in range(1, count):
+            pl.semaphore_signal(
+                barrier, inc=1, device_id={axis: lax.rem(me + step, count)}, device_id_type=MESH_ID
+            )
+    pl.semaphore_wait(barrier, sum(count - 1 for _, count, _ in axes))
+
+
+def send_all(axis, count, me, source, target, send_sems, recv_sems):
+    copies = []
+    for step in range(1, count):
+        peer = lax.rem(me + step, count)
+        copy = pltpu.make_async_remote_copy(
+            src_ref=source(peer),
+            dst_ref=target(step),
+            send_sem=send_sems.at[step - 1],
+            recv_sem=recv_sems.at[step - 1],
+            device_id={axis: peer},
+            device_id_type=MESH_ID,
+        )
+        copy.start()
+        copies.append(copy)
+    return copies
+
+
+def received(copies):
+    for copy in copies:
+        copy.wait_recv()
+
+
+def sent(copies):
+    for copy in copies:
+        copy.wait_send()
+
+
+def load_all(pairs, sems):
+    copies = [pltpu.make_async_copy(src, dst, sems.at[i]) for i, (src, dst) in enumerate(pairs)]
+    for copy in copies:
+        copy.start()
+    return copies
+
+
+def silu(value):
+    return value / (1.0 + jnp.exp(-value))
+
+
+def square_block(squares):
+    head = squares.astype(jnp.bfloat16).astype(jnp.float32)
+    rest = squares - head
+    lane = lax.broadcasted_iota(jnp.int32, (squares.shape[0], LANES), 1)
+    return jnp.where(lane < LANES // 2, head, rest).astype(jnp.bfloat16)
+
+
+def square_total(block):
+    return block[:, :1] + block[:, LANES // 2 : LANES // 2 + 1]
+
+
+def wide(ref):
+    return jnp.concatenate([ref[j] for j in range(ref.shape[0])], axis=1)
+
+
+def project_kernel(
+    n_kv, n_tp, features,
+    tokens, lengths, freq, gain, wq_hbm, wk_hbm, wv_hbm, wg_hbm,
+    qk_out, v_out, gate_out,
+    wq, wk, wv, wg, gathered, out_a, out_b, in_a, in_b,
+    load_sems, gs, gr, as_, ar, bs, br,
+):
+    kv, tp = lax.axis_index("kv"), lax.axis_index("tp")
+    loads = load_all([(wq_hbm, wq), (wk_hbm, wk), (wv_hbm, wv), (wg_hbm, wg)], load_sems)
+    greet([("tp", n_tp, tp), ("kv", n_kv, kv)])
+    copies = send_all("tp", n_tp, tp, lambda p: tokens, lambda s: gathered.at[tp], gs, gr)
+    gathered[tp] = tokens[...]
+    rows = out_a.shape[1]
+    row = lax.broadcasted_iota(jnp.int32, (rows, rows), 0)
+    col = lax.broadcasted_iota(jnp.int32, (rows, rows), 1)
+    spread = jnp.where(row == col, lengths[...].astype(jnp.float32), 0.0)
+    angles = jnp.sum(spread, axis=1, keepdims=True) * freq[...]
+    cosine, sine = jnp.cos(angles), jnp.sin(angles)
+    lane = lax.broadcasted_iota(jnp.int32, angles.shape, 1)
+    sine = jnp.where(lane < QK // 2, -sine, sine)
+    received(copies)
+    x = wide(gathered).astype(jnp.float32)
+    squares = jnp.sum(x * x, axis=1, keepdims=True)
+    normed = (x * gain[...]).astype(jnp.bfloat16)
+    q_width, v_width = wq.shape[1], wv.shape[1]
+
+    def project(weight):
+        full = jnp.dot(normed, weight[...], preferred_element_type=jnp.float32)
+        return full.astype(jnp.bfloat16).reshape(n_kv, rows, full.shape[1])
+
+    out_a[:, :, 2 * q_width :] = square_block(squares).reshape(n_kv, rows, LANES)
+    loads[0].wait()
+    out_a[:, :, :q_width] = project(wq)
+    loads[1].wait()
+    out_a[:, :, q_width : 2 * q_width] = project(wk)
+    first = send_all("kv", n_kv, kv, lambda p: out_a.at[p], lambda s: in_a.at[s - 1], as_, ar)
+    loads[2].wait()
+    out_b[:, :, :v_width] = project(wv)
+    loads[3].wait()
+    out_b[:, :, v_width:] = project(wg)
+    second = send_all("kv", n_kv, kv, lambda p: out_b.at[p], lambda s: in_b.at[s - 1], bs, br)
+    received(first)
+    total = out_a[kv].astype(jnp.float32)
+    for step in range(n_kv - 1):
+        total += in_a[step].astype(jnp.float32)
+    scale = lax.rsqrt(square_total(total[:, 2 * q_width :]) / features + 1e-06)
+    total = total * scale
+    blocks = []
+    for head in range(q_width // QK):
+        for base, factor in ((0, 1.0), (q_width, QK ** (-0.5))):
+            part = total[:, base + head * QK : base + (head + 1) * QK]
+            turned = (part * cosine + pltpu.roll(part, QK // 2, 1) * sine) * factor
+            blocks.append(turned.astype(jnp.bfloat16).astype(jnp.float32))
+    qk_out[...] = jnp.concatenate(blocks, axis=0).T
+    received(second)
+    total = out_b[kv].astype(jnp.float32)
+    for step in range(n_kv - 1):
+        total += in_b[step].astype(jnp.float32)
+    total = total * scale
+    v_out[...] = total[:, :v_width].astype(jnp.bfloat16).astype(jnp.float32)
+    gate_out[...] = silu(total[:, v_width:])
+    sent(copies)
+    sent(first)
+    sent(second)
+
+
+def state_kernel(n_tp, rows, qk, v, state, new_state, retained):
+    block, heads = state.shape[0], state.shape[1]
+    width = state.shape[3]
+    start = pl.program_id(0) * block
+    tp = lax.axis_index("tp")
+    turned = pltpu.roll(qk[...], lax.rem(LANES - start, LANES), 1)
+    for head in range(heads):
+        number = jnp.full((1, width), tp * heads + head, jnp.int32).astype(jnp.float32)
+        decay = 1.0 - jnp.exp2(-5.0 - 10.0 * number / (heads * n_tp - 1))
+        for s in range(block):
+            lane = 2 * head * rows + s
+            query = turned[:, lane : lane + 1]
+            key = turned[:, lane + rows : lane + rows + 1]
+            value = v[pl.ds(start + s, 1), head * width : (head + 1) * width]
+            new = decay * state[s, head] + key * value
+            new_state[s, head] = new
+            retained[pl.ds(start + s, 1), head * width : (head + 1) * width] = jnp.sum(
+                query * new, axis=0, keepdims=True
+            )
+
+
+def mix_kernel(
+    n_kv, n_tp, features, heads,
+    retained, gate, tokens, gain, wo_hbm, wg_hbm, wu_hbm, wd_hbm,
+    out,
+    wo, wg, wu, wd, merged, mixed_out, mixed_in, own, gathered,
+    up_out, gate_out, up_in, gate_in, hidden, down_out, down_in,
+    load_sems, ms, mr, xs, xr, cs, cr, as_, ar, bs, br, hs, hr, ds_, dr,
+):
+    kv, tp = lax.axis_index("kv"), lax.axis_index("tp")
+    loads = load_all([(wo_hbm, wo), (wg_hbm, wg), (wu_hbm, wu), (wd_hbm, wd)], load_sems)
+    rows = retained.shape[0]
+    width = retained.shape[1] // heads
+    parts = []
+    for head in range(heads):
+        part = retained[:, head * width : (head + 1) * width]
+        parts.append(part * lax.rsqrt(jnp.mean(part * part, axis=1, keepdims=True) + 1e-06))
+    merged[kv] = (jnp.concatenate(parts, axis=1) * gate[...]).astype(jnp.bfloat16)
+    greet([("tp", n_tp, tp), ("kv", n_kv, kv)])
+    copies_m = send_all("kv", n_kv, kv, lambda p: merged.at[kv], lambda s: merged.at[kv], ms, mr)
+    loads[0].wait()
+    received(copies_m)
+    batch = n_kv * rows
+    columns = tokens.shape[1]
+
+    def summed(lhs, weight, buffer_out, buffer_in, send_sems, recv_sems):
+        full = jnp.dot(lhs, weight[...], preferred_element_type=jnp.float32).astype(jnp.bfloat16)
+        for j in range(n_tp):
+            buffer_out[j] = full[:, j * columns : (j + 1) * columns]
+        copies = send_all(
+            "tp", n_tp, tp, lambda p: buffer_out.at[p], lambda s: buffer_in.at[s - 1], send_sems, recv_sems
+        )
+        received(copies)
+        total = buffer_out[tp].astype(jnp.float32)
+        for step in range(n_tp - 1):
+            total += buffer_in[step].astype(jnp.float32)
+        return total, copies
+
+    total, copies_x = summed(merged[...].reshape(batch, -1), wo, mixed_out, mixed_in, xs, xr)
+    residual = (tokens[...].astype(jnp.float32) + total).astype(jnp.bfloat16)
+    own[...] = residual
+    gathered[tp] = residual
+    copies_c = send_all("tp", n_tp, tp, lambda p: own, lambda s: gathered.at[tp], cs, cr)
+    received(copies_c)
+    x = wide(gathered).astype(jnp.float32)
+    squares = jnp.sum(x * x, axis=1, keepdims=True)
+    normed = (x * gain[...]).astype(jnp.bfloat16)
+    units = wg.shape[1]
+
+    def project(weight):
+        full = jnp.dot(normed, weight[...], preferred_element_type=jnp.float32)
+        return full.astype(jnp.bfloat16).reshape(n_kv, rows, full.shape[1])
+
+    gate_out[:, :, units:] = square_block(squares).reshape(n_kv, rows, LANES)
+    loads[1].wait()
+    gate_out[:, :, :units] = project(wg)
+    copies_a = send_all("kv", n_kv, kv, lambda p: gate_out.at[p], lambda s: gate_in.at[s - 1], as_, ar)
+    loads[2].wait()
+    up_out[...] = project(wu)
+    copies_b = send_all("kv", n_kv, kv, lambda p: up_out.at[p], lambda s: up_in.at[s - 1], bs, br)
+    received(copies_a)
+    total = gate_out[kv].astype(jnp.float32)
+    for step in range(n_kv - 1):
+        total += gate_in[step].astype(jnp.float32)
+    scale = lax.rsqrt(square_total(total[:, units:]) / features + 1e-06)
+    activated = silu(total[:, :units] * scale)
+    received(copies_b)
+    total = up_out[kv].astype(jnp.float32)
+    for step in range(n_kv - 1):
+        total += up_in[step].astype(jnp.float32)
+    hidden[kv] = (activated * (total * scale)).astype(jnp.bfloat16)
+    copies_h = send_all("kv", n_kv, kv, lambda p: hidden.at[kv], lambda s: hidden.at[kv], hs, hr)
+    loads[3].wait()
+    received(copies_h)
+    total, copies_d = summed(hidden[...].reshape(batch, units), wd, down_out, down_in, ds_, dr)
+    out[...] = (own[...].astype(jnp.float32) + total).astype(jnp.bfloat16)
+    for copies in (copies_m, copies_x, copies_c, copies_a, copies_b, copies_h, copies_d):
+        sent(copies)
+
+
+def fused_on_device(n_kv, n_tp, *arrays):
+    (
+        tokens, lengths, state, mixer_gain, wq, wk, wv, wg, wo, channel_gain, fg, fu, fd,
+    ) = arrays
+    batch, columns = tokens.shape
+    rows, heads, _, width = state.shape
+    depth, q_width = wq.shape
+    v_width, units = wv.shape[1], fg.shape[1]
+    features = depth * n_kv
+    bf16, f32 = jnp.bfloat16, jnp.float32
+    vmem = pl.BlockSpec(memory_space=pltpu.VMEM)
+    hbm = pl.BlockSpec(memory_space=pltpu.HBM)
+    dma = pltpu.SemaphoreType.DMA
+    tp_sems, kv_sems = [dma((n_tp - 1,))] * 2, [dma((n_kv - 1,))] * 2
+    index = np.arange(QK) % (QK // 2)
+    freq = jnp.asarray((10000.0 ** (-index / (QK // 2))).astype(np.float32))[None, :]
+    a_width, b_width = 2 * q_width + LANES, 2 * v_width
+    qk, value, gate = pl.pallas_call(
+        functools.partial(project_kernel, n_kv, n_tp, features),
+        out_shape=(
+            jax.ShapeDtypeStruct((QK, LANES), f32),
+            jax.ShapeDtypeStruct((rows, v_width), f32),
+            jax.ShapeDtypeStruct((rows, v_width), f32),
+        ),
+        in_specs=[vmem] * 4 + [hbm] * 4,
+        out_specs=(vmem,) * 3,
+        scratch_shapes=[
+            pltpu.VMEM(wq.shape, bf16),
+            pltpu.VMEM(wk.shape, bf16),
+            pltpu.VMEM(wv.shape, bf16),
+            pltpu.VMEM(wg.shape, bf16),
+            pltpu.VMEM((n_tp, batch, columns), bf16),
+            pltpu.VMEM((n_kv, rows, a_width), bf16),
+            pltpu.VMEM((n_kv, rows, b_width), bf16),
+            pltpu.VMEM((n_kv - 1, rows, a_width), bf16),
+            pltpu.VMEM((n_kv - 1, rows, b_width), bf16),
+            dma((4,)),
+        ]
+        + tp_sems + kv_sems + kv_sems,
+        compiler_params=pltpu.CompilerParams(
+            collective_id=0, has_side_effects=True, vmem_limit_bytes=VMEM_LIMIT
+        ),
+        name="project",
+    )(tokens, lengths[None, :], freq, mixer_gain[None, :], wq, wk, wv, wg)
+
+    block = 4
+    state_spec = pl.BlockSpec((block, heads, QK, width), lambda i: (i, 0, 0, 0))
+    new_state, retained = pl.pallas_call(
+        functools.partial(state_kernel, n_tp, rows),
+        grid=(rows // block,),
+        out_shape=(
+            jax.ShapeDtypeStruct(state.shape, f32),
+            jax.ShapeDtypeStruct((rows, v_width), f32),
+        ),
+        in_specs=[
+            pl.BlockSpec((QK, LANES), lambda i: (0, 0)),
+            pl.BlockSpec((rows, v_width), lambda i: (0, 0)),
+            state_spec,
+        ],
+        out_specs=(state_spec, pl.BlockSpec((rows, v_width), lambda i: (0, 0))),
+        compiler_params=pltpu.CompilerParams(vmem_limit_bytes=VMEM_LIMIT),
+        name="state",
+    )(qk, value, state)
+
+    layer_output = pl.pallas_call(
+        functools.partial(mix_kernel, n_kv, n_tp, features, heads),
+        out_shape=jax.ShapeDtypeStruct(tokens.shape, bf16),
+        in_specs=[vmem] * 4 + [hbm] * 4,
+        out_specs=vmem,
+        scratch_shapes=[
+            pltpu.VMEM(wo.shape, bf16),
+            pltpu.VMEM(fg.shape, bf16),
+            pltpu.VMEM(fu.shape, bf16),
+            pltpu.VMEM(fd.shape, bf16),
+            pltpu.VMEM((n_kv, rows, v_width), bf16),
+            pltpu.VMEM((n_tp, batch, columns), bf16),
+            pltpu.VMEM((n_tp - 1, batch, columns), bf16),
+            pltpu.VMEM((batch, columns), bf16),
+            pltpu.VMEM((n_tp, batch, columns), bf16),
+            pltpu.VMEM((n_kv, rows, units), bf16),
+            pltpu.VMEM((n_kv, rows, units + LANES), bf16),
+            pltpu.VMEM((n_kv - 1, rows, units), bf16),
+            pltpu.VMEM((n_kv - 1, rows, units + LANES), bf16),
+            pltpu.VMEM((n_kv, rows, units), bf16),
+            pltpu.VMEM((n_tp, batch, columns), bf16),
+            pltpu.VMEM((n_tp - 1, batch, columns), bf16),
+            dma((4,)),
+        ]
+        + kv_sems + tp_sems + tp_sems + kv_sems + kv_sems + kv_sems + tp_sems,
+        compiler_params=pltpu.CompilerParams(
+            collective_id=1, has_side_effects=True, vmem_limit_bytes=VMEM_LIMIT
+        ),
+        name="mix",
+    )(retained, gate, tokens, channel_gain[None, :], wo, fg, fu, fd)
+    return layer_output, new_state
+
+
+def fits(n_kv, n_tp, arrays):
+    tokens, state, ffn_gate = arrays[0], arrays[2], arrays[10]
+    rows, heads = state.shape[0], state.shape[1]
+    return (
+        tokens.shape[1] % LANES == 0
+        and ffn_gate.shape[1] % LANES == 0
+        and rows % 16 == 0
+        and 2 * heads * rows == LANES
+        and state.shape[2] == QK == LANES
+        and state.shape[3] % LANES == 0
+    )
+
+
+def per_device(n_kv, n_tp, *arrays):
+    if fits(n_kv, n_tp, arrays):
+        return fused_on_device(n_kv, n_tp, *arrays)
+    return on_device(*arrays)
+
+
 def solution(mesh):
     in_specs = (
         P(None, ("kv", "tp")),
@@ -155,5 +510,6 @@
     )
     out_specs = (P(None, ("kv", "tp")), P("kv", "tp", None, None))
     return jax.shard_map(
-        on_device, mesh=mesh, in_specs=in_specs, out_specs=out_specs, check_vma=False
-    )
+        functools.partial(per_device, mesh.shape["kv"], mesh.shape["tp"]),
+        mesh=mesh, in_specs=in_specs, out_specs=out_specs, check_vma=False
+    )

time: 210 us -> 82.6 us (0.39)
  waiting for transfers between devices: 111 us -> 0 us
  Pallas kernels: 0 us -> 73.5 us
  blocking collectives: 57.1 us -> 0 us
  between operations: 14.7 us -> 0.71 us
  matrix products: 11.2 us -> 0 us
  other arithmetic: 10.4 us -> 0 us
  local copies, waits for them, and re-layouts: 4.66 us -> 7.92 us
    pallas_call x0 -> x3, Pallas kernels: none -> 73.5 us  [the longest x1 43.4 us: fused_on_device(): pl.pallas_call(functools.partial(mix_kernel, n_kv, n_tp, features, heads)...]
    unnamed x6 -> x0, waiting for transfers between devices: 61.9 us -> none
    all_gather x3 -> x0, blocking collectives: 36.9 us -> none  [the longest x2 28.4 us: gathered_rows(): return lax.all_gather(columns, 'tp', axis=1, tiled=True)]
    psum x1 -> x0, waiting for transfers between devices: 35.9 us -> none  [every_sum(): lax.psum(partial_value.astype(jnp.bfloat16), 'kv').astype(jnp.float32)]
    reduce_scatter x1 -> x0, waiting for transfers between devices: 13 us -> none  [owned_sums(): lax.psum_scatter(partial_value.astype(jnp.bfloat16), 'kv', scatter_dimens...]
    dot_general x9 -> x0, matrix products: 11.2 us -> none  [the longest x1 2.83 us: on_device(): jnp.einsum('bhk,bhkv->bhv', query_rows.astype(jnp.float32), new_state, pr...]
    psum x1 -> x0, blocking collectives: 10.2 us -> none  [every_sum(): lax.psum(squares.astype(jnp.bfloat16), 'kv').astype(jnp.float32)]
    unnamed x1 -> x0, blocking collectives: 9.95 us -> none
  transfers between devices with their start and end apart: 4 -> 0, of which waited for: 4 -> 0; matrix products, arithmetic and copies ran while one was open for 1% -> 0% of each run, Pallas kernels for 0% -> 0%
where the time goes in v1:
time: 82.6 us; the launch traced here: 82.1 us
  Pallas kernels  73.5 us (89%)
  local copies, waits for them, and re-layouts  7.92 us (10%)
    pallas_call x1, Pallas kernels, fused_on_device(): pl.pallas_call(functools.partial(mix_kernel, n_kv, n_tp, features, heads)...  43.4 us
    pallas_call x1, Pallas kernels, fused_on_device(): pl.pallas_call(functools.partial(project_kernel, n_kv, n_tp, features), o...  19.5 us
    pallas_call x1, Pallas kernels, fused_on_device(): pl.pallas_call(functools.partial(state_kernel, n_tp, rows), grid=(rows //...  10.6 us
    unnamed x25, local copies, waits for them, and re-layouts  7.92 us

profile of v1, /device:TPU:0, one launch (start us, length us, event | category | flops | bytes accessed | tf_op | source)
XLA Modules:
  0.0 82.1 jit_solution(4005786366510984338)
XLA Ops:
  0.6 0.0 copy-start.1
  0.6 1.2 %copy-done.1 = bf16[1024,512]{1,0:T(8,128)(2,1)S(1)} copy-done((bf16[1024,512]{1,0:T(8,128)(2,1)S(1)}, bf16[1024,512]{1,0:T(8,128)(2,1)}, u32[]{:S(2)}) %copy-start.1) | copy-done | bytes 1048600
  1.9 0.0 copy-start.2
  1.9 1.2 %copy-done.2 = bf16[1024,512]{1,0:T(8,128)(2,1)S(1)} copy-done((bf16[1024,512]{1,0:T(8,128)(2,1)S(1)}, bf16[1024,512]{1,0:T(8,128)(2,1)}, u32[]{:S(2)}) %copy-start.2) | copy-done | bytes 1048600
  3.1 0.0 copy-start.4
  3.1 1.0 %copy-done.4 = bf16[1024,256]{1,0:T(8,128)(2,1)S(1)} copy-done((bf16[1024,256]{1,0:T(8,128)(2,1)S(1)}, bf16[1024,256]{1,0:T(8,128)(2,1)}, u32[]{:S(2)}) %copy-start.4) | copy-done | bytes 524312
  4.1 0.0 copy-start.5
  4.1 1.0 %copy-done.5 = bf16[1024,256]{1,0:T(8,128)(2,1)S(1)} copy-done((bf16[1024,256]{1,0:T(8,128)(2,1)S(1)}, bf16[1024,256]{1,0:T(8,128)(2,1)}, u32[]{:S(2)}) %copy-start.5) | copy-done | bytes 524312
  5.2 0.0 copy-start.6
  5.2 0.8 copy-done.6
  5.9 0.0 copy-start.8
  5.9 0.7 copy-done.8
  6.6 0.0 copy-start.10
  6.6 0.7 copy-done.10
  7.3 0.0 copy-start.11
  7.3 0.7 copy-done.11
  7.9 19.5 %project.1 = (f32[128,128]{1,0:T(8,128)S(1)}, f32[32,512]{1,0:T(8,128)S(1)}, f32[32,512]{1,0:T(8,128)S(1)}) custom-call(bf16[128,128]{1,0:T(8,128)(2,1)S(1)} %copy-done.6, s32[1,32]{1,0:T(1,128)S(1)} %bitcast.5, f32[1,128]{1,0:T(1,128)S(1)} %copy-done.11, f32[1,1024]{1,0:T(1,128)S(1)} %bitcast.3, bf16[1024,256]{1,0:T(8,128)(2,1)S(1)} %copy-done.4, ...), custom_call_target="tpu_custom_call" | custom-call | tf_op jit(solution)/shard_map/project/pallas_call | solution.py:396
  27.4 0.0 copy-start
  27.4 0.0 copy-start.3
  27.5 0.0 copy-start.7
  27.5 0.0 copy-start.9
  27.5 10.6 %state.2 = (f32[32,2,128,256]{3,2,1,0:T(8,128)}, f32[32,512]{1,0:T(8,128)S(1)}) custom-call(f32[128,128]{1,0:T(8,128)S(1)} %get-tuple-element.7.qk, f32[32,512]{1,0:T(8,128)S(1)} %get-tuple-element.8.v, f32[32,2,128,256]{3,2,1,0:T(8,128)} %state.3), custom_call_target="tpu_custom_call" | custom-call | tf_op jit(solution)/shard_map/state/pallas_call | solution.py:426
  38.1 0.0 copy-done
  38.1 0.0 copy-done.3
  38.1 0.0 copy-done.7
  38.1 0.0 copy-done.9
  38.1 43.4 %mix.1 = bf16[128,128]{1,0:T(8,128)(2,1)S(1)} custom-call(f32[32,512]{1,0:T(8,128)S(1)} %get-tuple-element.9.retained, f32[32,512]{1,0:T(8,128)S(1)} %get-tuple-element.10.gate, bf16[128,128]{1,0:T(8,128)(2,1)S(1)} %copy-done.7, f32[1,1024]{1,0:T(1,128)S(1)} %bitcast.4, bf16[512,1024]{1,0:T(8,128)(2,1)S(1)} %copy-done.3, bf16[1024,1408]{1,0:T(8,128)(2,1)S(1)} %copy-done, ...), custom_call_target="tpu_custom_call" | custom-call | tf_op jit(solution)/shard_map/mix/pallas_call | solution.py:443
  81.5 0.6 copy.17
Async XLA Ops:
  0.6 1.2 %copy-start.1 = (bf16[1024,512]{1,0:T(8,128)(2,1)S(1)}, bf16[1024,512]{1,0:T(8,128)(2,1)}, u32[]{:S(2)}) copy-start(bf16[1024,512]{1,0:T(8,128)(2,1)} %wv_hbm.1) | copy-start | bytes 3145732
  1.9 1.2 %copy-start.2 = (bf16[1024,512]{1,0:T(8,128)(2,1)S(1)}, bf16[1024,512]{1,0:T(8,128)(2,1)}, u32[]{:S(2)}) copy-start(bf16[1024,512]{1,0:T(8,128)(2,1)} %wg_hbm.2) | copy-start | bytes 3145732
  3.1 1.0 %copy-start.4 = (bf16[1024,256]{1,0:T(8,128)(2,1)S(1)}, bf16[1024,256]{1,0:T(8,128)(2,1)}, u32[]{:S(2)}) copy-start(bf16[1024,256]{1,0:T(8,128)(2,1)} %wq_hbm.1) | copy-start | bytes 1572868
  4.1 1.0 %copy-start.5 = (bf16[1024,256]{1,0:T(8,128)(2,1)S(1)}, bf16[1024,256]{1,0:T(8,128)(2,1)}, u32[]{:S(2)}) copy-start(bf16[1024,256]{1,0:T(8,128)(2,1)} %wk_hbm.1) | copy-start | bytes 1572868
  5.2 0.8 copy-start.6
  5.9 0.7 copy-start.8
  6.6 0.7 copy-start.10
  7.3 0.7 copy-start.11
  27.4 10.7 %copy-start = (bf16[1024,1408]{1,0:T(8,128)(2,1)S(1)}, bf16[1024,1408]{1,0:T(8,128)(2,1)}, u32[]{:S(2)}) copy-start(bf16[1024,1408]{1,0:T(8,128)(2,1)} %wg_hbm.3) | copy-start | bytes 8650756
  27.4 10.6 %copy-start.3 = (bf16[512,1024]{1,0:T(8,128)(2,1)S(1)}, bf16[512,1024]{1,0:T(8,128)(2,1)}, u32[]{:S(2)}) copy-start(bf16[512,1024]{1,0:T(8,128)(2,1)} %wo_hbm.1) | copy-start | bytes 3145732
  27.5 10.6 %copy-start.7 = (bf16[128,128]{1,0:T(8,128)(2,1)S(1)}, bf16[128,128]{1,0:T(8,128)(2,1)}, u32[]{:S(2)}) copy-start(bf16[128,128]{1,0:T(8,128)(2,1)} %tokens.3) | copy-start | bytes 98308
  27.5 10.6 %copy-start.9 = (f32[1024]{0:T(1024)S(1)}, f32[1024]{0:T(1024)}, u32[]{:S(2)}) copy-start(f32[1024]{0:T(1024)} %param.23) | copy-start | bytes 12292

commit v2 on v0

--- a/solution.py
+++ b/solution.py
@@ -1,11 +1,17 @@
+import functools
+
 import jax
 import jax.numpy as jnp
+import numpy as np
 from jax import lax
+from jax.experimental import pallas as pl
+from jax.experimental.pallas import tpu as pltpu
 from jax.sharding import PartitionSpec as P
 
 D = 4096
 HEADS = 16
 QK = 128
+LANES = 128
 
 
 def rotate_heads(vectors, positions):
@@ -137,6 +143,405 @@
     return (layer_output, new_state)
 
 
+MESH_ID = pl.DeviceIdType.MESH
+VMEM_TOTAL = 67043328
+CORES = 2
+
+
+def greet(groups):
+    barrier = pltpu.get_barrier_semaphore()
+    for axis, peers in groups:
+        for peer in peers:
+            pl.semaphore_signal(barrier, inc=1, device_id={axis: peer}, device_id_type=MESH_ID)
+    pl.semaphore_wait(barrier, sum(len(peers) for _, peers in groups))
+
+
+def send_all(axis, count, me, source, target, send_sems, recv_sems):
+    copies = []
+    for step in range(1, count):
+        peer = lax.rem(me + step, count)
+        copy = pltpu.make_async_remote_copy(
+            src_ref=source(peer),
+            dst_ref=target(step),
+            send_sem=send_sems.at[step - 1],
+            recv_sem=recv_sems.at[step - 1],
+            device_id={axis: peer},
+            device_id_type=MESH_ID,
+        )
+        copy.start()
+        copies.append(copy)
+    return copies
+
+
+def received(copies):
+    for copy in copies:
+        copy.wait_recv()
+
+
+def sent(copies):
+    for copy in copies:
+        copy.wait_send()
+
+
+def load_all(pairs, sems):
+    copies = [pltpu.make_async_copy(src, dst, sems.at[i]) for i, (src, dst) in enumerate(pairs)]
+    for copy in copies:
+        copy.start()
+    return copies
+
+
+def silu(value):
+    return value / (1.0 + jnp.exp(-value))
+
+
+def square_block(squares):
+    head = squares.astype(jnp.bfloat16).astype(jnp.float32)
+    rest = squares - head
+    lane = lax.broadcasted_iota(jnp.int32, (squares.shape[0], LANES), 1)
+    return jnp.where(lane < LANES // 2, head, rest).astype(jnp.bfloat16)
+
+
+def square_total(block):
+    return block[:, :1] + block[:, LANES // 2 : LANES // 2 + 1]
+
+
+def wide(ref):
+    return jnp.concatenate([ref[j] for j in range(ref.shape[0])], axis=1)
+
+
+def remote(axis, peer, source, target, send_sem, recv_sem):
+    return pltpu.make_async_remote_copy(
+        src_ref=source, dst_ref=target, send_sem=send_sem, recv_sem=recv_sem,
+        device_id={axis: peer}, device_id_type=MESH_ID,
+    )
+
+
+def gather_tp(slots, source, tp, n_tp, send_sems, recv_sems):
+    chips = n_tp // CORES
+    chip, core = tp // CORES, lax.rem(tp, CORES)
+    partner = chip * CORES + 1 - core
+    direct = []
+    for step in range(1, chips):
+        peer = lax.rem(chip + step, chips) * CORES + core
+        direct.append(
+            remote("tp", peer, source, slots.at[tp], send_sems.at[step], recv_sems.at[step])
+        )
+    across = [remote("tp", partner, source, slots.at[tp], send_sems.at[0], recv_sems.at[0])]
+    for copy in direct + across:
+        copy.start()
+
+    def finish():
+        for step in range(1, chips):
+            direct[step - 1].wait_recv()
+            slot = lax.rem(chip - step + chips, chips) * CORES + core
+            i = chips - 1 + step
+            copy = remote(
+                "tp", partner, slots.at[slot], slots.at[slot], send_sems.at[i], recv_sems.at[i]
+            )
+            copy.start()
+            across.append(copy)
+        received(across)
+        return direct + across
+
+    return finish
+
+
+def reduce_tp(lhs, weight, parts, swapped, staged, landed, tp, n_tp, send_sems, recv_sems):
+    chips = n_tp // CORES
+    chip, core = tp // CORES, lax.rem(tp, CORES)
+    partner = chip * CORES + 1 - core
+    columns = parts.shape[3]
+    full = jnp.dot(lhs, weight[...], preferred_element_type=jnp.float32).astype(jnp.bfloat16)
+    for j in range(n_tp):
+        parts[j % CORES, j // CORES] = full[:, j * columns : (j + 1) * columns]
+    swap = remote(
+        "tp", partner, parts.at[1 - core], swapped, send_sems.at[0], recv_sems.at[0]
+    )
+    swap.start()
+    swap.wait_recv()
+    copies = []
+    for step in range(1, chips):
+        other = lax.rem(chip + step, chips)
+        pair = parts[core, other].astype(jnp.float32) + swapped[other].astype(jnp.float32)
+        staged[step - 1] = pair.astype(jnp.bfloat16)
+        copy = remote(
+            "tp", other * CORES + core, staged.at[step - 1], landed.at[step - 1],
+            send_sems.at[step], recv_sems.at[step],
+        )
+        copy.start()
+        copies.append(copy)
+    total = parts[core, chip].astype(jnp.float32) + swapped[chip].astype(jnp.float32)
+    for step in range(1, chips):
+        copies[step - 1].wait_recv()
+        total += landed[step - 1].astype(jnp.float32)
+    return total, copies + [swap]
+
+
+def total_of(own, landed):
+    total = own.astype(jnp.float32)
+    for step in range(landed.shape[0]):
+        total += landed[step].astype(jnp.float32)
+    return total
+
+
+def layer_kernel(
+    n_kv, n_tp, features,
+    tokens_hbm, lengths_hbm, freq_hbm, gain_hbm, gain_two_hbm, state_hbm,
+    wq_hbm, wk_hbm, wv_hbm, wg_hbm, wo_hbm, fg_hbm, fu_hbm, fd_hbm,
+    out, state_out,
+    state, lengths, freq, gain, gain_two, wq, wk, wv, wg, wo, fg, fu, fd,
+    gathered, out_a, out_b, in_a, in_b, qk, value, retained, merged,
+    parts_x, swapped_x, staged_x, landed_x, own, gathered_two,
+    gate_out, up_out, gate_in, up_in, hidden, parts_d, swapped_d, staged_d, landed_d,
+    load_sems, store_sem, gs, gr, as_, ar, bs, br, ms, mr, xs, xr, cs, cr, es, er, fs, fr, hs, hr, ds_, dr,
+):
+    kv, tp = lax.axis_index("kv"), lax.axis_index("tp")
+    chips = n_tp // CORES
+    chip, core = tp // CORES, lax.rem(tp, CORES)
+    pairs = [
+        (tokens_hbm, gathered.at[tp]), (lengths_hbm, lengths), (freq_hbm, freq), (gain_hbm, gain),
+        (wq_hbm, wq), (wk_hbm, wk), (wv_hbm, wv), (wg_hbm, wg), (state_hbm, state),
+        (gain_two_hbm, gain_two), (wo_hbm, wo), (fg_hbm, fg), (fu_hbm, fu), (fd_hbm, fd),
+    ]
+    loads = load_all(pairs, load_sems)
+    along = [lax.rem(chip + step, chips) * CORES + core for step in range(1, chips)]
+    greet([
+        ("tp", along + [chip * CORES + 1 - core]),
+        ("kv", [lax.rem(kv + step, n_kv) for step in range(1, n_kv)]),
+    ])
+    loads[0].wait()
+    finish_g = gather_tp(gathered, gathered.at[tp], tp, n_tp, gs, gr)
+    for i in (1, 2, 3):
+        loads[i].wait()
+    rows = out_a.shape[1]
+    row = lax.broadcasted_iota(jnp.int32, (rows, rows), 0)
+    col = lax.broadcasted_iota(jnp.int32, (rows, rows), 1)
+    spread = jnp.where(row == col, lengths[...].astype(jnp.float32), 0.0)
+    angles = jnp.sum(spread, axis=1, keepdims=True) * freq[...]
+    cosine, sine = jnp.cos(angles), jnp.sin(angles)
+    lane = lax.broadcasted_iota(jnp.int32, angles.shape, 1)
+    sine = jnp.where(lane < QK // 2, -sine, sine)
+    started = finish_g()
+
+    def normalise(slots, gains):
+        x = wide(slots).astype(jnp.float32)
+        squares = jnp.sum(x * x, axis=1, keepdims=True)
+        return (x * gains[...]).astype(jnp.bfloat16), square_block(squares).reshape(n_kv, rows, LANES)
+
+    def project(lhs, weight):
+        full = jnp.dot(lhs, weight[...], preferred_element_type=jnp.float32)
+        return full.astype(jnp.bfloat16).reshape(n_kv, rows, full.shape[1])
+
+    normed, squares = normalise(gathered, gain)
+    q_width, v_width = wq.shape[1], wv.shape[1]
+    heads = q_width // QK
+    width = v_width // heads
+    out_a[:, :, 2 * q_width :] = squares
+    loads[4].wait()
+    out_a[:, :, :q_width] = project(normed, wq)
+    loads[5].wait()
+    out_a[:, :, q_width : 2 * q_width] = project(normed, wk)
+    first = send_all("kv", n_kv, kv, lambda p: out_a.at[p], lambda s: in_a.at[s - 1], as_, ar)
+    loads[6].wait()
+    out_b[:, :, :v_width] = project(normed, wv)
+    loads[7].wait()
+    out_b[:, :, v_width:] = project(normed, wg)
+    second = send_all("kv", n_kv, kv, lambda p: out_b.at[p], lambda s: in_b.at[s - 1], bs, br)
+    loads[8].wait()
+    received(first)
+    total = total_of(out_a[kv], in_a)
+    scale = lax.rsqrt(square_total(total[:, 2 * q_width :]) / features + 1e-06)
+    total = total * scale
+    blocks = []
+    for base, factor in ((0, 1.0), (q_width, QK ** (-0.5))):
+        for head in range(heads):
+            part = total[:, base + head * QK : base + (head + 1) * QK]
+            turned = (part * cosine + pltpu.roll(part, QK // 2, 1) * sine) * factor
+            blocks.append(turned.astype(jnp.bfloat16).astype(jnp.float32))
+    qk[...] = jnp.concatenate(blocks, axis=0).T
+    block = 4
+
+    def turned_to(start):
+        return pltpu.roll(qk[...], lax.rem(LANES - start, LANES), 1)
+
+    def query_step(i, carry):
+        start = i * block
+        turned = turned_to(start)
+        for s in range(block):
+            for head in range(heads):
+                query = turned[:, head * rows + s : head * rows + s + 1]
+                retained[pl.ds(start + s, 1), head * width : (head + 1) * width] = jnp.sum(
+                    query * state[start + s, head], axis=0, keepdims=True
+                )
+        return carry
+
+    lax.fori_loop(0, rows // block, query_step, 0)
+    decays = []
+    for head in range(heads):
+        number = jnp.full((1, width), tp * heads + head, jnp.int32).astype(jnp.float32)
+        decays.append(1.0 - jnp.exp2(-5.0 - 10.0 * number / (heads * n_tp - 1)))
+    received(second)
+    total = total_of(out_b[kv], in_b) * scale
+    value[...] = total[:, :v_width].astype(jnp.bfloat16).astype(jnp.float32)
+    pieces = []
+    for head in range(heads):
+        overlap = jnp.sum(blocks[head] * blocks[heads + head], axis=1, keepdims=True)
+        span = slice(head * width, (head + 1) * width)
+        piece = decays[head] * retained[:, span] + overlap * value[:, span]
+        pieces.append(piece * lax.rsqrt(jnp.mean(piece * piece, axis=1, keepdims=True) + 1e-06))
+    merged[kv] = (jnp.concatenate(pieces, axis=1) * silu(total[:, v_width:])).astype(jnp.bfloat16)
+    copies_m = send_all("kv", n_kv, kv, lambda p: merged.at[kv], lambda s: merged.at[kv], ms, mr)
+
+    def update_step(i, carry):
+        start = i * block
+        turned = turned_to(start)
+        for s in range(block):
+            for head in range(heads):
+                lane = (heads + head) * rows + s
+                outer = turned[:, lane : lane + 1] * value[pl.ds(start + s, 1), head * width : (head + 1) * width]
+                state[start + s, head] = decays[head] * state[start + s, head] + outer
+        return carry
+
+    lax.fori_loop(0, rows // block, update_step, 0)
+    loads[10].wait()
+    received(copies_m)
+    store = pltpu.make_async_copy(state, state_out, store_sem)
+    store.start()
+    batch = n_kv * rows
+    total, copies_x = reduce_tp(
+        merged[...].reshape(batch, v_width), wo, parts_x, swapped_x, staged_x, landed_x, tp, n_tp, xs, xr
+    )
+    residual = (tokens_of(gathered, tp) + total).astype(jnp.bfloat16)
+    own[...] = residual
+    gathered_two[tp] = residual
+    finish_c = gather_tp(gathered_two, own, tp, n_tp, cs, cr)
+    loads[9].wait()
+    loads[11].wait()
+    copies_c = finish_c()
+    normed, squares = normalise(gathered_two, gain_two)
+    units = fg.shape[1]
+    gate_out[:, :, units:] = squares
+    gate_out[:, :, :units] = project(normed, fg)
+    copies_e = send_all("kv", n_kv, kv, lambda p: gate_out.at[p], lambda s: gate_in.at[s - 1], es, er)
+    loads[12].wait()
+    up_out[...] = project(normed, fu)
+    copies_f = send_all("kv", n_kv, kv, lambda p: up_out.at[p], lambda s: up_in.at[s - 1], fs, fr)
+    received(copies_e)
+    total = total_of(gate_out[kv], gate_in)
+    scale = lax.rsqrt(square_total(total[:, units:]) / features + 1e-06)
+    activated = silu(total[:, :units] * scale)
+    received(copies_f)
+    hidden[kv] = (activated * (total_of(up_out[kv], up_in) * scale)).astype(jnp.bfloat16)
+    copies_h = send_all("kv", n_kv, kv, lambda p: hidden.at[kv], lambda s: hidden.at[kv], hs, hr)
+    loads[13].wait()
+    received(copies_h)
+    total, copies_d = reduce_tp(
+        hidden[...].reshape(batch, units), fd, parts_d, swapped_d, staged_d, landed_d, tp, n_tp, ds_, dr
+    )
+    out[...] = (own[...].astype(jnp.float32) + total).astype(jnp.bfloat16)
+    for copies in (started, first, second, copies_m, copies_x, copies_c, copies_e, copies_f, copies_h, copies_d):
+        sent(copies)
+    store.wait()
+
+
+def tokens_of(slots, tp):
+    return slots[tp].astype(jnp.float32)
+
+
+def fused_on_device(n_kv, n_tp, *arrays):
+    (
+        tokens, lengths, state, mixer_gain, wq, wk, wv, wg, wo, channel_gain, fg, fu, fd,
+    ) = arrays
+    batch, columns = tokens.shape
+    rows = state.shape[0]
+    depth, q_width = wq.shape
+    v_width, units = wv.shape[1], fg.shape[1]
+    bf16, f32 = jnp.bfloat16, jnp.float32
+    vmem = pl.BlockSpec(memory_space=pltpu.VMEM)
+    hbm = pl.BlockSpec(memory_space=pltpu.HBM)
+    dma = pltpu.SemaphoreType.DMA
+    tp_sems, kv_sems = [dma((n_tp - 1,))] * 2, [dma((n_kv - 1,))] * 2
+    chips = n_tp // CORES
+    chip_sems = [dma((chips,))] * 2
+    index = np.arange(QK) % (QK // 2)
+    freq = jnp.asarray((10000.0 ** (-index / (QK // 2))).astype(np.float32))[None, :]
+    a_width, b_width = 2 * q_width + LANES, 2 * v_width
+    reduce_scratch = [
+        pltpu.VMEM((CORES, chips, batch, columns), bf16),
+        pltpu.VMEM((chips, batch, columns), bf16),
+        pltpu.VMEM((chips - 1, batch, columns), bf16),
+        pltpu.VMEM((chips - 1, batch, columns), bf16),
+    ]
+    return pl.pallas_call(
+        functools.partial(layer_kernel, n_kv, n_tp, depth * n_kv),
+        out_shape=(
+            jax.ShapeDtypeStruct(tokens.shape, bf16),
+            jax.ShapeDtypeStruct(state.shape, f32),
+        ),
+        in_specs=[hbm] * 14,
+        out_specs=(vmem, hbm),
+        scratch_shapes=[
+            pltpu.VMEM(state.shape, f32),
+            pltpu.VMEM((1, rows), jnp.int32),
+            pltpu.VMEM((1, QK), f32),
+            pltpu.VMEM((1, depth), f32),
+            pltpu.VMEM((1, depth), f32),
+        ]
+        + [pltpu.VMEM(w.shape, bf16) for w in (wq, wk, wv, wg, wo, fg, fu, fd)]
+        + [
+            pltpu.VMEM((n_tp, batch, columns), bf16),
+            pltpu.VMEM((n_kv, rows, a_width), bf16),
+            pltpu.VMEM((n_kv, rows, b_width), bf16),
+            pltpu.VMEM((n_kv - 1, rows, a_width), bf16),
+            pltpu.VMEM((n_kv - 1, rows, b_width), bf16),
+            pltpu.VMEM((QK, LANES), f32),
+            pltpu.VMEM((rows, v_width), f32),
+            pltpu.VMEM((rows, v_width), f32),
+            pltpu.VMEM((n_kv, rows, v_width), bf16),
+        ]
+        + reduce_scratch
+        + [
+            pltpu.VMEM((batch, columns), bf16),
+            pltpu.VMEM((n_tp, batch, columns), bf16),
+            pltpu.VMEM((n_kv, rows, units + LANES), bf16),
+            pltpu.VMEM((n_kv, rows, units), bf16),
+            pltpu.VMEM((n_kv - 1, rows, units + LANES), bf16),
+            pltpu.VMEM((n_kv - 1, rows, units), bf16),
+            pltpu.VMEM((n_kv, rows, units), bf16),
+        ]
+        + reduce_scratch
+        + [dma((14,)), dma]
+        + tp_sems + kv_sems + kv_sems + kv_sems + chip_sems + tp_sems + kv_sems + kv_sems + kv_sems + chip_sems,
+        compiler_params=pltpu.CompilerParams(
+            collective_id=0, has_side_effects=True, vmem_limit_bytes=VMEM_TOTAL
+        ),
+        name="layer",
+    )(tokens, lengths[None, :], freq, mixer_gain[None, :], channel_gain[None, :], state, wq, wk, wv, wg, wo, fg, fu, fd)
+
+
+def fits(n_kv, n_tp, arrays):
+    tokens, state, ffn_gate = arrays[0], arrays[2], arrays[10]
+    rows, heads = state.shape[0], state.shape[1]
+    return (
+        tokens.shape[1] % LANES == 0
+        and n_tp % CORES == 0
+        and n_tp > CORES
+        and n_kv > 1
+        and 4 * state.size < VMEM_TOTAL // 4
+        and ffn_gate.shape[1] % LANES == 0
+        and rows % 16 == 0
+        and 2 * heads * rows == LANES
+        and state.shape[2] == QK == LANES
+        and state.shape[3] % LANES == 0
+    )
+
+
+def per_device(n_kv, n_tp, *arrays):
+    if fits(n_kv, n_tp, arrays):
+        return fused_on_device(n_kv, n_tp, *arrays)
+    return on_device(*arrays)
+
+
 def solution(mesh):
     in_specs = (
         P(None, ("kv", "tp")),
@@ -155,5 +560,6 @@
     )
     out_specs = (P(None, ("kv", "tp")), P("kv", "tp", None, None))
     return jax.shard_map(
-        on_device, mesh=mesh, in_specs=in_specs, out_specs=out_specs, check_vma=False
-    )
+        functools.partial(per_device, mesh.shape["kv"], mesh.shape["tp"]),
+        mesh=mesh, in_specs=in_specs, out_specs=out_specs, check_vma=False
+    )

time: 210 us -> 67.3 us (0.32)
  waiting for transfers between devices: 111 us -> 0 us
  Pallas kernels: 0 us -> 57.3 us
  blocking collectives: 57.1 us -> 0 us
  between operations: 14.7 us -> 0.64 us
  matrix products: 11.2 us -> 0 us
  other arithmetic: 10.4 us -> 0 us
  local copies, waits for them, and re-layouts: 4.66 us -> 9.15 us
    unnamed x6 -> x0, waiting for transfers between devices: 61.9 us -> none
    pallas_call x0 -> x1, Pallas kernels: none -> 57.3 us  [fused_on_device(): pl.pallas_call(functools.partial(layer_kernel, n_kv, n_tp, depth * n_kv),...]
    all_gather x3 -> x0, blocking collectives: 36.9 us -> none  [the longest x2 28.4 us: gathered_rows(): return lax.all_gather(columns, 'tp', axis=1, tiled=True)]
    psum x1 -> x0, waiting for transfers between devices: 35.9 us -> none  [every_sum(): lax.psum(partial_value.astype(jnp.bfloat16), 'kv').astype(jnp.float32)]
    reduce_scatter x1 -> x0, waiting for transfers between devices: 13 us -> none  [owned_sums(): lax.psum_scatter(partial_value.astype(jnp.bfloat16), 'kv', scatter_dimens...]
    dot_general x9 -> x0, matrix products: 11.2 us -> none  [the longest x1 2.83 us: on_device(): jnp.einsum('bhk,bhkv->bhv', query_rows.astype(jnp.float32), new_state, pr...]
    psum x1 -> x0, blocking collectives: 10.2 us -> none  [every_sum(): lax.psum(squares.astype(jnp.bfloat16), 'kv').astype(jnp.float32)]
    unnamed x1 -> x0, blocking collectives: 9.95 us -> none
  transfers between devices with their start and end apart: 4 -> 0, of which waited for: 4 -> 0; matrix products, arithmetic and copies ran while one was open for 1% -> 0% of each run, Pallas kernels for 0% -> 0%
where the time goes in v2:
time: 67.3 us; the launch traced here: 67.1 us
  Pallas kernels  57.3 us (85%)
  local copies, waits for them, and re-layouts  9.15 us (14%)
    pallas_call x1, Pallas kernels, fused_on_device(): pl.pallas_call(functools.partial(layer_kernel, n_kv, n_tp, depth * n_kv),...  57.3 us
    unnamed x2, local copies, waits for them, and re-layouts  9.15 us

profile of v2, /device:TPU:0, one launch (start us, length us, event | category | flops | bytes accessed | tf_op | source)
XLA Modules:
  0.0 67.1 jit_solution(7053371861008458500)
XLA Ops:
  0.6 57.3 %layer.1 = (bf16[128,128]{1,0:T(8,128)(2,1)}, f32[32,2,128,256]{3,2,1,0:T(8,128)}) custom-call(bf16[128,128]{1,0:T(8,128)(2,1)} %tokens_hbm.1, s32[1,32]{1,0:T(1,128)} %bitcast.5, f32[1,128]{1,0:T(1,128)} %constant.4.freq_hbm, f32[1,1024]{1,0:T(1,128)} %bitcast.3, f32[1,1024]{1,0:T(1,128)} %bitcast.4, f32[32,2,128,256]{3,2,1,0:T(8,128)} %state_hbm.1, ...), custom_call_target="tpu_custom_call" | custom-call | tf_op jit(solution)/shard_map/layer/pallas_call | solution.py:475
  57.9 1.4 %copy.18 = bf16[128,128]{1,0:T(8,128)(2,1)} copy(bf16[128,128]{1,0:T(8,128)(2,1)} %get-tuple-element.4) | data formatting | bytes 65536
  59.3 7.8 %copy.19 = f32[32,2,128,256]{3,2,1,0:T(8,128)} copy(f32[32,2,128,256]{3,2,1,0:T(8,128)} %get-tuple-element.5) | data formatting | bytes 16777216

commit v3 on v2

--- a/solution.py
+++ b/solution.py
@@ -251,13 +251,20 @@
     chip, core = tp // CORES, lax.rem(tp, CORES)
     partner = chip * CORES + 1 - core
     columns = parts.shape[3]
-    full = jnp.dot(lhs, weight[...], preferred_element_type=jnp.float32).astype(jnp.bfloat16)
-    for j in range(n_tp):
-        parts[j % CORES, j // CORES] = full[:, j * columns : (j + 1) * columns]
+
+    def multiply(side):
+        starts = [pl.multiple_of((z * CORES + side) * columns, LANES) for z in range(chips)]
+        rhs = jnp.concatenate([weight[:, pl.ds(start, columns)] for start in starts], axis=1)
+        full = jnp.dot(lhs, rhs, preferred_element_type=jnp.float32).astype(jnp.bfloat16)
+        for z in range(chips):
+            parts[side, z] = full[:, z * columns : (z + 1) * columns]
+
+    multiply(1 - core)
     swap = remote(
         "tp", partner, parts.at[1 - core], swapped, send_sems.at[0], recv_sems.at[0]
     )
     swap.start()
+    multiply(core)
     swap.wait_recv()
     copies = []
     for step in range(1, chips):
@@ -444,6 +451,23 @@
     store.wait()
 
 
+def finish_kernel(state, out, state_to, out_to, slots, small, load_sems, store_sems):
+    chunks, size = slots.shape[0], slots.shape[1]
+    pairs, targets = [(out, small)], [(small, out_to)]
+    for i in range(chunks):
+        pairs.append((state.at[pl.ds(i * size, size)], slots.at[i]))
+        targets.append((slots.at[i], state_to.at[pl.ds(i * size, size)]))
+    loads = load_all(pairs, load_sems)
+    stores = []
+    for i, (source, target) in enumerate(targets):
+        loads[i].wait()
+        copy = pltpu.make_async_copy(source, target, store_sems.at[i])
+        copy.start()
+        stores.append(copy)
+    for copy in stores:
+        copy.wait()
+
+
 def tokens_of(slots, tp):
     return slots[tp].astype(jnp.float32)
 
@@ -472,7 +496,7 @@
         pltpu.VMEM((chips - 1, batch, columns), bf16),
         pltpu.VMEM((chips - 1, batch, columns), bf16),
     ]
-    return pl.pallas_call(
+    out, new_state = pl.pallas_call(
         functools.partial(layer_kernel, n_kv, n_tp, depth * n_kv),
         out_shape=(
             jax.ShapeDtypeStruct(tokens.shape, bf16),
@@ -517,6 +541,25 @@
         ),
         name="layer",
     )(tokens, lengths[None, :], freq, mixer_gain[None, :], channel_gain[None, :], state, wq, wk, wv, wg, wo, fg, fu, fd)
+    chunks = 8
+    new_state, out = pl.pallas_call(
+        finish_kernel,
+        out_shape=(
+            jax.ShapeDtypeStruct(state.shape, f32),
+            jax.ShapeDtypeStruct(tokens.shape, bf16),
+        ),
+        in_specs=[hbm, hbm],
+        out_specs=(hbm, hbm),
+        scratch_shapes=[
+            pltpu.VMEM((chunks, rows // chunks) + state.shape[1:], f32),
+            pltpu.VMEM(tokens.shape, bf16),
+            dma((chunks + 1,)),
+            dma((chunks + 1,)),
+        ],
+        compiler_params=pltpu.CompilerParams(vmem_limit_bytes=VMEM_TOTAL),
+        name="finish",
+    )(new_state, out)
+    return out, new_state
 
 
 def fits(n_kv, n_tp, arrays):

time: 67.3 us -> 64.6 us (0.960)
  local copies, waits for them, and re-layouts: 9.15 us -> 0 us
  Pallas kernels: 57.3 us -> 63.8 us
    unnamed x2 -> x0, local copies, waits for them, and re-layouts: 9.15 us -> none
    pallas_call x0 -> x1, Pallas kernels: none -> 6.47 us  [fused_on_device(): pl.pallas_call(finish_kernel, out_shape=(jax.ShapeDtypeStruct(state.shape...]
where the time goes in v3:
time: 64.6 us; the launch traced here: 64.5 us
  Pallas kernels  63.8 us (99%)
    pallas_call x1, Pallas kernels, fused_on_device(): pl.pallas_call(functools.partial(layer_kernel, n_kv, n_tp, depth * n_kv),...  57.4 us
    pallas_call x1, Pallas kernels, fused_on_device(): pl.pallas_call(finish_kernel, out_shape=(jax.ShapeDtypeStruct(state.shape...  6.47 us

profile of v3, /device:TPU:0, one launch (start us, length us, event | category | flops | bytes accessed | tf_op | source)
XLA Modules:
  0.0 64.5 jit_solution(7229478742108584692)
XLA Ops:
  0.6 57.4 %layer.1 = (bf16[128,128]{1,0:T(8,128)(2,1)}, f32[32,2,128,256]{3,2,1,0:T(8,128)}) custom-call(bf16[128,128]{1,0:T(8,128)(2,1)} %tokens_hbm.1, s32[1,32]{1,0:T(1,128)} %bitcast.5, f32[1,128]{1,0:T(1,128)} %constant.4.freq_hbm, f32[1,1024]{1,0:T(1,128)} %bitcast.3, f32[1,1024]{1,0:T(1,128)} %bitcast.4, f32[32,2,128,256]{3,2,1,0:T(8,128)} %state_hbm.1, ...), custom_call_target="tpu_custom_call" | custom-call | tf_op jit(solution)/shard_map/layer/pallas_call | solution.py:499
  58.0 6.5 %finish.1 = (f32[32,2,128,256]{3,2,1,0:T(8,128)}, bf16[128,128]{1,0:T(8,128)(2,1)}) custom-call(f32[32,2,128,256]{3,2,1,0:T(8,128)} %get-tuple-element.6.state, bf16[128,128]{1,0:T(8,128)(2,1)} %get-tuple-element.7.out), custom_call_target="tpu_custom_call" | custom-call | tf_op jit(solution)/shard_map/finish/pallas_call | solution.py:545
